TPU v7x, 128 devices: a whole 4x4x4 slice. The times are simulated.
128 devices in a mesh: fs: 16 (over z, y), tp: 8 (over x, core).
Axes of the slice: x: 4, y: 4, z: 4, core: 2. Of those that a mesh axis runs over, the one named last changes fastest.
Arguments:
- weights_in: float32 [2, 2048, 5632], P(None, 'fs', 'tp'), may hold values from -6 to 6
- weights_mix: float32 [2048, 2048], P('fs', 'tp'), may hold values from -6 to 6
- momentum_in: float32 [2, 2048, 5632], P(None, 'fs', 'tp'), may hold values from -5 to 5
- momentum_mix: float32 [2048, 2048], P('fs', 'tp'), may hold values from -5 to 5
- grads_in: float32 [2, 2048, 5632], P(None, 'fs', 'tp'), may hold values from -5 to 5
- grads_mix: float32 [2048, 2048], P('fs', 'tp'), may hold values from -5 to 5
Outputs:
- momentum_in_next: float32 [2, 2048, 5632], P(None, 'fs', 'tp')
- momentum_mix_next: float32 [2048, 2048], P('fs', 'tp')
- weights_in_next: float32 [2, 2048, 5632], P(None, 'fs', 'tp')
- weights_mix_next: float32 [2048, 2048], P('fs', 'tp')
- update_in: float32 [2, 2048, 5632], P(None, 'fs', 'tp')
- update_mix: float32 [2048, 2048], P('fs', 'tp')
All inputs are finite; a program needn't handle non-finite values.
Results may differ from a plain program's by a relative error of at most 0.0003.
Values sent between devices are 32-bit elements; how exact they have to be, the bound alone decides.
No kernel may reach another device: no remote copies, remote signals or barrier semaphores. Data moves between devices by JAX's collectives and lax.ppermute only.
A program may use at most 128 MiB of HBM per device.

v0:
```python
import math
import jax
import jax.numpy as jnp
from jax import lax
from jax.sharding import PartitionSpec as P

D = 2048
FF = 5632
ITERS = 3
A_COEF = 3.4445
B_COEF = -4.775
C_COEF = 2.0315
MOMENTUM_DECAY = 0.95
STEP_RATE = 0.02
HIGH = lax.Precision.HIGHEST


def gather_turned(arrays, axis, dims):
    turned = [jnp.moveaxis(a, dim, 0) for a, dim in zip(arrays, dims)]
    both = jnp.concatenate([t.reshape(len(t), -1) for t in turned], axis=1)
    result, at, gathered = (lax.all_gather(both, axis, axis=0, tiled=True), 0, [])
    for t, dim in zip(turned, dims):
        share = result[:, at : at + t[0].size].reshape(-1, *t.shape[1:])
        gathered.append(jnp.moveaxis(share, 0, dim))
        at += t[0].size
    return tuple(gathered)


def rows_for(lines, peers):
    spare = -lines.shape[0] % peers
    if not spare:
        return lines
    return jnp.concatenate([lines, jnp.zeros((spare, *lines.shape[1:]), lines.dtype)])


def sum_by_parts(shard, axis):
    lines = shard.reshape(-1, *shard.shape[1:][-1:])
    own = lax.psum_scatter(
        rows_for(lines, lax.axis_size(axis)), axis, scatter_dimension=0, tiled=True
    )
    whole = lax.all_gather(own, axis).reshape(-1, *lines.shape[1:])
    return lax.slice_in_dim(whole, 0, len(lines)).reshape(shard.shape)


def scale_from(summed):
    return (0.5 * lax.rsqrt(jnp.maximum(summed / D, 1.0)))[:, None, None]


def block_trace(shard, row_start, col_start):
    row_ids = row_start + lax.iota(jnp.int32, shard.shape[1])[:, None]
    col_ids = col_start + lax.iota(jnp.int32, shard.shape[2])[None, :]
    return jnp.sum(jnp.where((row_ids == col_ids)[None], shard, 0.0), axis=(1, 2))


def local(weights_in, weights_mix, momentum_in, momentum_mix, grads_in, grads_mix):
    fs_pos = lax.axis_index("fs")
    tp_pos = lax.axis_index("tp")
    moment_in = MOMENTUM_DECAY * momentum_in + grads_in
    moment_mix = MOMENTUM_DECAY * momentum_mix + grads_mix
    local_in = moment_in
    local_mix = moment_mix[None]
    row_count = local_in.shape[1]
    block_width = local_mix.shape[2]
    for iteration in range(ITERS):
        cols_in, cols_mix = gather_turned((local_in, local_mix), "fs", (1, 1))
        partial_value = jnp.concatenate(
            [
                jnp.einsum("krc,ksc->krs", local_in, cols_in, precision=HIGH),
                jnp.einsum("krc,ksc->krs", local_mix, cols_mix, precision=HIGH),
            ]
        )
        gram_rows = sum_by_parts(partial_value, "tp")
        gram_block = lax.dynamic_slice_in_dim(gram_rows, tp_pos * block_width, block_width, 2)
        if iteration == 0:
            traces = block_trace(gram_block, fs_pos * row_count, tp_pos * block_width)
            scaling = scale_from(lax.psum(traces, ("fs", "tp")))
        factor = scaling if iteration == 0 else jnp.ones_like(scaling)
        gram_cols = lax.all_gather(gram_block, "fs", axis=1, tiled=True)
        square = jnp.einsum("krs,ksc->krc", gram_rows, gram_cols, precision=HIGH)
        poly_mat = factor**2 * B_COEF * gram_block + factor**4 * C_COEF * square
        poly_rows = lax.all_gather(poly_mat, "tp", axis=2, tiled=True)
        local_in = factor[:2] * (
            A_COEF * local_in + jnp.einsum("krs,ksc->krc", poly_rows[:2], cols_in, precision=HIGH)
        )
        local_mix = factor[2:] * (
            A_COEF * local_mix + jnp.einsum("krs,ksc->krc", poly_rows[2:], cols_mix, precision=HIGH)
        )
    step_in = local_in * math.sqrt(max(D, FF))
    step_mix = local_mix[0] * math.sqrt(D)
    return (
        moment_in,
        moment_mix,
        weights_in - STEP_RATE * step_in,
        weights_mix - STEP_RATE * step_mix,
        step_in,
        step_mix,
    )


def solution(mesh):
    in_specs = (
        P(None, "fs", "tp"),
        P("fs", "tp"),
        P(None, "fs", "tp"),
        P("fs", "tp"),
        P(None, "fs", "tp"),
        P("fs", "tp"),
    )
    out_specs = (
        P(None, "fs", "tp"),
        P("fs", "tp"),
        P(None, "fs", "tp"),
        P("fs", "tp"),
        P(None, "fs", "tp"),
        P("fs", "tp"),
    )
    return jax.shard_map(local, mesh=mesh, in_specs=in_specs, out_specs=out_specs, check_vma=False)
```

profile of v0, /device:TPU:1, one launch (start us, length us, event | category | flops | bytes accessed | tf_op | source)
XLA Modules:
  0.0 954.7 jit_solution(4597433947635089846)
XLA Ops:
  7.2 1.0 multiply_add_fusion.1
  8.3 1.4 multiply_add_fusion
  9.7 1.1 pad_maximum_fusion.3
  10.9 105.9 %all-gather.16.cloned.1.call-done = f32[2048,1664]{0,1:T(8,128)} async-done(((f32[128,1664]{0,1:T(8,128)}), f32[2048,1664]{0,1:T(8,128)}) %all-gather.16.cloned.1.call-update) | async-done | bytes 13631504 | tf_op jit(solution)/shard_map/all_gather | solution.py:21
  116.8 10.4 %slice.58 = f32[2048,1408]{0,1:T(8,128)} slice(f32[2048,1664]{0,1:T(8,128)} %all-gather.16.cloned.1.call-done), slice={[0:2048], [0:1408]} | slice | bytes 23068672 | tf_op jit(solution)/shard_map/slice | solution.py:23
  127.2 9.2 fusion.25
  136.4 2.8 convolution_bitcast_fusion.2
  139.2 1.9 pad_maximum_fusion
  141.2 33.7 %reduce-scatter.4.cloned.1.call-done = f32[48,2048]{1,0:T(8,128)} async-done(((f32[384,2048]{1,0:T(8,128)}), f32[48,2048]{1,0:T(8,128)}) %reduce-scatter.4.cloned.1.call-update) | async-done | bytes 393232 | tf_op jit(solution)/shard_map/reduce_scatter | solution.py:38
  175.1 31.3 %all-gather.34.cloned.1.call-done = f32[384,2048]{1,0:T(8,128)} async-done(((f32[48,2048]{1,0:T(8,128)}), f32[384,2048]{1,0:T(8,128)}) %all-gather.34.cloned.1.call-update) | async-done | bytes 3145744 | tf_op jit(solution)/shard_map/all_gather | solution.py:41
  206.4 1.8 select_reduce_fusion
  208.3 67.5 %psum.7 = f32[3]{0:T(128)S(1)} all-reduce(f32[3]{0:T(128)S(1)} %get-tuple-element.8), channel_id=1, replica_groups=mesh['fs'=16,'tp'=8] {'fs','tp'}, use_global_device_ids=true, to_apply=%region_2.3 | all-reduce | flops 3 | bytes 24 | tf_op jit(solution)/shard_map/psum | solution.py:76
  275.8 8.2 fusion.10
  284.1 0.2 all-gather.22.cloned.1.call-start
  284.3 0.6 slice.48
  284.9 23.8 %all-gather.20.cloned.1.call-done = f32[3,128,2048]{2,1,0:T(8,128)} async-done(((f32[3,128,256]{2,1,0:T(8,128)}), f32[3,128,2048]{2,1,0:T(8,128)}) %all-gather.20.cloned.1.call-update) | async-done | bytes 3145744 | tf_op jit(solution)/shard_map/all_gather | solution.py:81
  308.7 4.8 fusion.16
  313.6 13.0 %fusion.9 = f32[2,128,704]{1,2,0:T(8,128)S(1)} fusion(f32[3,128,2048]{2,1,0:T(8,128)} %all-gather.20.cloned.1.call-done, f32[2,2048,704]{1,2,0:T(8,128)} %bitcast.65, f32[2,128,704]{1,2,0:T(8,128)S(1)} %multiply_add_fusion, f32[2]{0:T(128)S(1)} %bitcast.82), kind=kOutput, calls=%fused_computation.18 | convolution fusion | flops 4429725696 | bytes 16121864 | tf_op jit(solution)/shard_map/krs,ksc->krc/dot_general | solution.py:83
  326.6 1.0 pad_maximum_fusion.4
  327.6 0.3 reduce-scatter.6.cloned.1.call-start
  327.9 102.1 %all-gather.22.cloned.1.call-done = f32[2048,1664]{0,1:T(8,128)} async-done(((f32[128,1664]{0,1:T(8,128)}), f32[2048,1664]{0,1:T(8,128)}) %all-gather.22.cloned.1.call-update) | async-done | bytes 13631504 | tf_op jit(solution)/shard_map/all_gather | solution.py:21
  429.9 10.4 %slice.61 = f32[2048,1408]{0,1:T(8,128)} slice(f32[2048,1664]{0,1:T(8,128)} %all-gather.22.cloned.1.call-done), slice={[0:2048], [0:1408]} | slice | bytes 23068672 | tf_op jit(solution)/shard_map/slice | solution.py:23
  440.3 9.2 fusion.26
  449.5 2.8 convolution_bitcast_fusion.1
  452.3 1.9 pad_maximum_fusion.1
  454.4 33.7 %reduce-scatter.6.cloned.1.call-done = f32[48,2048]{1,0:T(8,128)} async-done(((f32[384,2048]{1,0:T(8,128)}), f32[48,2048]{1,0:T(8,128)}) %reduce-scatter.6.cloned.1.call-update) | async-done | bytes 393232 | tf_op jit(solution)/shard_map/reduce_scatter | solution.py:38
  488.1 31.5 %all-gather.36.cloned.1.call-done = f32[384,2048]{1,0:T(8,128)} async-done(((f32[48,2048]{1,0:T(8,128)}), f32[384,2048]{1,0:T(8,128)}) %all-gather.36.cloned.1.call-update) | async-done | bytes 3145744 | tf_op jit(solution)/shard_map/all_gather | solution.py:41
  519.6 1.8 constant_dynamic-slice_fusion.1
  521.4 61.7 %all-gather.24.cloned.1.call-done = f32[3,2048,256]{2,1,0:T(8,128)} async-done(((f32[3,128,256]{2,1,0:T(8,128)}), f32[3,2048,256]{2,1,0:T(8,128)}) %all-gather.24.cloned.1.call-update) | async-done | bytes 6291472 | tf_op jit(solution)/shard_map/all_gather | solution.py:78
  583.1 8.2 fusion.11
  591.3 0.4 all-gather.28.cloned.1.call-start
  591.8 27.5 %all-gather.26.cloned.1.call-done = f32[3,128,2048]{2,1,0:T(8,128)} async-done(((f32[3,128,256]{2,1,0:T(8,128)}), f32[3,128,2048]{2,1,0:T(8,128)}) %all-gather.26.cloned.1.call-update) | async-done | bytes 3145744 | tf_op jit(solution)/shard_map/all_gather | solution.py:81
  619.3 4.1 fusion.19
  623.5 13.0 %convolution_add_fusion.1 = f32[2,128,704]{1,2,0:T(8,128)S(1)} fusion(f32[3,128,2048]{2,1,0:T(8,128)} %all-gather.26.cloned.1.call-done, f32[2,2048,704]{1,2,0:T(8,128)} %bitcast.69, f32[2,128,704]{1,2,0:T(8,128)S(1)} %fusion.9), kind=kOutput, calls=%fused_computation.16 | convolution fusion | flops 4429545472 | bytes 16121856 | tf_op jit(solution)/shard_map/krs,ksc->krc/dot_general | solution.py:83
  636.5 1.0 pad_maximum_fusion.5
  637.6 102.3 %all-gather.28.cloned.1.call-done = f32[2048,1664]{0,1:T(8,128)} async-done(((f32[128,1664]{0,1:T(8,128)}), f32[2048,1664]{0,1:T(8,128)}) %all-gather.28.cloned.1.call-update) | async-done | bytes 13631504 | tf_op jit(solution)/shard_map/all_gather | solution.py:21
  739.8 10.4 %slice.64 = f32[2048,1408]{0,1:T(8,128)} slice(f32[2048,1664]{0,1:T(8,128)} %all-gather.28.cloned.1.call-done), slice={[0:2048], [0:1408]} | slice | bytes 23068672 | tf_op jit(solution)/shard_map/slice | solution.py:23
  750.2 9.2 fusion.27
  759.4 2.8 convolution_bitcast_fusion
  762.2 1.9 pad_maximum_fusion.2
  764.2 33.7 %reduce-scatter.8.cloned.1.call-done = f32[48,2048]{1,0:T(8,128)} async-done(((f32[384,2048]{1,0:T(8,128)}), f32[48,2048]{1,0:T(8,128)}) %reduce-scatter.8.cloned.1.call-update) | async-done | bytes 393232 | tf_op jit(solution)/shard_map/reduce_scatter | solution.py:38
  798.0 31.5 %all-gather.38.cloned.1.call-done = f32[384,2048]{1,0:T(8,128)} async-done(((f32[48,2048]{1,0:T(8,128)}), f32[384,2048]{1,0:T(8,128)}) %all-gather.38.cloned.1.call-update) | async-done | bytes 3145744 | tf_op jit(solution)/shard_map/all_gather | solution.py:41
  829.5 1.8 constant_dynamic-slice_fusion
  831.5 61.4 %all-gather.30.cloned.1.call-done = f32[3,2048,256]{2,1,0:T(8,128)} async-done(((f32[3,128,256]{2,1,0:T(8,128)}), f32[3,2048,256]{2,1,0:T(8,128)}) %all-gather.30.cloned.1.call-update) | async-done | bytes 6291472 | tf_op jit(solution)/shard_map/all_gather | solution.py:78
  892.8 8.2 fusion.12
  901.1 27.9 %all-gather.32.cloned.1.call-done = f32[3,128,2048]{2,1,0:T(8,128)} async-done(((f32[3,128,256]{2,1,0:T(8,128)}), f32[3,128,2048]{2,1,0:T(8,128)}) %all-gather.32.cloned.1.call-update) | async-done | bytes 3145744 | tf_op jit(solution)/shard_map/all_gather | solution.py:81
  929.0 5.0 broadcast_multiply_fusion.1
  934.0 13.9 %broadcast_multiply_fusion = (f32[2,128,704]{1,2,0:T(8,128)}, f32[2,128,704]{1,2,0:T(8,128)}) fusion(f32[2,128,704]{1,2,0:T(8,128)S(1)} %copy-done.3, f32[3,128,2048]{2,1,0:T(8,128)S(1)} %copy-done.1, f32[2,2048,704]{1,2,0:T(8,128)} %bitcast.67, f32[2,128,704]{1,2,0:T(8,128)S(1)} %convolution_add_fusion.1), kind=kOutput, calls=%fused_computation.38 | convolution fusion | flops 4430086144 | bytes 17563648 | tf_op jit(solution)/shard_map/krs,ksc->krc/dot_general | solution.py:83
  (46 shorter events, 1.3 us)
Async XLA Ops:
  7.2 109.6 %all-gather.16.cloned.1.call-start = ((), (), s32[]{:S(2)}) async-start(), calls=%async_computation.3 | async-start | bytes 14483456 | tf_op jit(solution)/shard_map/all_gather | solution.py:21
  8.2 300.5 %copy-start.2 = (f32[128,256]{1,0:T(8,128)}, f32[128,256]{1,0:T(8,128)S(1)}, u32[]{:S(2)}) copy-start(f32[128,256]{1,0:T(8,128)S(1)} %multiply_add_fusion.1) | copy-start | bytes 393220
  9.7 303.9 %copy-start = (f32[2,128,704]{1,2,0:T(8,128)}, f32[2,128,704]{1,2,0:T(8,128)S(1)}, u32[]{:S(2)}) copy-start(f32[2,128,704]{1,2,0:T(8,128)S(1)} %multiply_add_fusion) | copy-start | bytes 2162692
  10.8 164.1 %reduce-scatter.4.cloned.1.call-start = ((), (), s32[]{:S(2)}) async-start(), calls=%async_computation.4 | async-start | bytes 3538944 | tf_op jit(solution)/shard_map/reduce_scatter | solution.py:38
  141.2 65.3 %all-gather.34.cloned.1.call-start = ((), (), s32[]{:S(2)}) async-start(), calls=%async_computation.15 | async-start | bytes 3538944 | tf_op jit(solution)/shard_map/all_gather | solution.py:41
  174.9 100.9 %all-gather.18.cloned.1.call-start = ((), (), s32[]{:S(2)}) async-start(), calls=%async_computation.5 | async-start | bytes 6684672 | tf_op jit(solution)/shard_map/all_gather | solution.py:78
  208.2 100.5 %all-gather.20.cloned.1.call-start = ((), (), s32[]{:S(2)}) async-start(), calls=%async_computation.6 | async-start | bytes 3538944 | tf_op jit(solution)/shard_map/all_gather | solution.py:81
  284.1 145.9 %all-gather.22.cloned.1.call-start = ((), (), s32[]{:S(2)}) async-start(), calls=%async_computation.7 | async-start | bytes 14483456 | tf_op jit(solution)/shard_map/all_gather | solution.py:21
  327.6 160.4 %reduce-scatter.6.cloned.1.call-start = ((), (), s32[]{:S(2)}) async-start(), calls=%async_computation.8 | async-start | bytes 3538944 | tf_op jit(solution)/shard_map/reduce_scatter | solution.py:38
  454.3 65.3 %all-gather.36.cloned.1.call-start = ((), (), s32[]{:S(2)}) async-start(), calls=%async_computation.16 | async-start | bytes 3538944 | tf_op jit(solution)/shard_map/all_gather | solution.py:41
  488.1 95.1 %all-gather.24.cloned.1.call-start = ((), (), s32[]{:S(2)}) async-start(), calls=%async_computation.9 | async-start | bytes 6684672 | tf_op jit(solution)/shard_map/all_gather | solution.py:78
  521.4 97.9 %all-gather.26.cloned.1.call-start = ((), (), s32[]{:S(2)}) async-start(), calls=%async_computation.10 | async-start | bytes 3538944 | tf_op jit(solution)/shard_map/all_gather | solution.py:81
  591.3 148.5 %all-gather.28.cloned.1.call-start = ((), (), s32[]{:S(2)}) async-start(), calls=%async_computation.11 | async-start | bytes 14483456 | tf_op jit(solution)/shard_map/all_gather | solution.py:21
  637.5 160.4 %reduce-scatter.8.cloned.1.call-start = ((), (), s32[]{:S(2)}) async-start(), calls=%async_computation.12 | async-start | bytes 3538944 | tf_op jit(solution)/shard_map/reduce_scatter | solution.py:38
  764.2 65.3 %all-gather.38.cloned.1.call-start = ((), (), s32[]{:S(2)}) async-start(), calls=%async_computation.17 | async-start | bytes 3538944 | tf_op jit(solution)/shard_map/all_gather | solution.py:41
  797.9 94.9 %all-gather.30.cloned.1.call-start = ((), (), s32[]{:S(2)}) async-start(), calls=%async_computation.13 | async-start | bytes 6684672 | tf_op jit(solution)/shard_map/all_gather | solution.py:78
  831.2 97.8 %copy-start.4 = (f32[128,256]{1,0:T(8,128)S(1)}, f32[128,256]{1,0:T(8,128)}, u32[]{:S(2)}) copy-start(f32[128,256]{1,0:T(8,128)} %param.7) | copy-start | bytes 393220
  831.3 97.8 %all-gather.32.cloned.1.call-start = ((), (), s32[]{:S(2)}) async-start(), calls=%async_computation.14 | async-start | bytes 3538944 | tf_op jit(solution)/shard_map/all_gather | solution.py:81
  901.1 33.0 %copy-start.3 = (f32[2,128,704]{1,2,0:T(8,128)S(1)}, f32[2,128,704]{1,2,0:T(8,128)}, u32[]{:S(2)}) copy-start(f32[2,128,704]{1,2,0:T(8,128)} %param.6) | copy-start | bytes 2162692
  929.0 5.0 copy-start.1
Sparse Core Ops, SparseCore 0:
  10.9 105.7 all-gather.15
  141.3 33.5 reduce-scatter.3
  176.6 29.8 all-gather.33
  209.0 61.3 all-gather.17
  284.2 24.4 all-gather.19
  327.7 102.1 all-gather.21
  454.4 33.5 reduce-scatter.5
  489.7 29.8 all-gather.35
  522.3 60.7 all-gather.23
  591.5 27.7 all-gather.25
  637.6 102.1 all-gather.27
  764.3 33.5 reduce-scatter.7
  799.6 29.8 all-gather.37
  832.0 60.7 all-gather.29
  901.2 27.7 all-gather.31
where the time goes:
time: 963 us; the launch traced here: 955 us
  waiting for transfers between devices  708 us (74%)
  matrix products  114 us (12%)
  blocking collectives  67.5 us (7%)
  local copies, waits for them, and re-layouts  35.7 us (4%)
  between operations  14.3 us (1%)
  other arithmetic  13.1 us (1%)
    all_gather x3, waiting for transfers between devices, gather_turned(): lax.all_gather(both, axis, axis=0, tiled=True)  310 us
    all_gather x3, waiting for transfers between devices, local(): gram_cols = lax.all_gather(gram_block, 'fs', axis=1, tiled=True)  123 us
    reduce_scatter x3, waiting for transfers between devices, sum_by_parts(): lax.psum_scatter(rows_for(lines, lax.axis_size(axis)), axis, scatter_dime...  101 us
    all_gather x3, waiting for transfers between devices, sum_by_parts(): whole = lax.all_gather(own, axis).reshape(-1, *lines.shape[1:])  94.3 us
    all_gather x3, waiting for transfers between devices, local(): poly_rows = lax.all_gather(poly_mat, 'tp', axis=2, tiled=True)  79.3 us
    psum x1, blocking collectives, local(): scaling = scale_from(lax.psum(traces, ('fs', 'tp')))  67.5 us
    dot_general x3, matrix products, local(): jnp.einsum('krs,ksc->krc', poly_rows[:2], cols_in, precision=HIGH)  39.9 us
    slice x3, local copies, waits for them, and re-layouts, gather_turned(): share = result[:, at:at + t[0].size].reshape(-1, *t.shape[1:])  31.2 us
  transfers between devices with their start and end apart: 15, of which 14 were waited for; matrix products, arithmetic and copies ran while one was open for 0% of the time, Pallas kernels for 0%

commit v1 on v0

--- a/solution.py
+++ b/solution.py
@@ -78,7 +78,8 @@
         gram_cols = lax.all_gather(gram_block, "fs", axis=1, tiled=True)
         square = jnp.einsum("krs,ksc->krc", gram_rows, gram_cols, precision=HIGH)
         poly_mat = factor**2 * B_COEF * gram_block + factor**4 * C_COEF * square
-        poly_rows = lax.all_gather(poly_mat, "tp", axis=2, tiled=True)
+        terms = lax.all_gather(poly_mat, "tp", axis=0, tiled=False)
+        poly_rows = jnp.concatenate(terms, axis=2)
         local_in = factor[:2] * (
             A_COEF * local_in + jnp.einsum("krs,ksc->krc", poly_rows[:2], cols_in, precision=HIGH)
         )

time: 963 us -> 975 us (1.012)
  local copies, waits for them, and re-layouts: 35.7 us -> 51.1 us
    slice x0 -> x9, local copies, waits for them, and re-layouts: none -> 10.2 us  [the longest x6 8.15 us: local(): poly_rows[2:]]
where the time goes in v1:
time: 975 us; the launch traced here: 966 us
  waiting for transfers between devices  708 us (73%)
  matrix products  110 us (11%)
  blocking collectives  67.5 us (7%)
  local copies, waits for them, and re-layouts  51.1 us (5%)
  between operations  14.6 us (1%)
  other arithmetic  13.1 us (1%)
    all_gather x3, waiting for transfers between devices, gather_turned(): lax.all_gather(both, axis, axis=0, tiled=True)  310 us
    all_gather x3, waiting for transfers between devices, local(): gram_cols = lax.all_gather(gram_block, 'fs', axis=1, tiled=True)  123 us
    reduce_scatter x3, waiting for transfers between devices, sum_by_parts(): lax.psum_scatter(rows_for(lines, lax.axis_size(axis)), axis, scatter_dime...  101 us
    all_gather x3, waiting for transfers between devices, sum_by_parts(): whole = lax.all_gather(own, axis).reshape(-1, *lines.shape[1:])  94.3 us
    all_gather x3, waiting for transfers between devices, local(): terms = lax.all_gather(poly_mat, 'tp', axis=0, tiled=False)  79.5 us
    psum x1, blocking collectives, local(): scaling = scale_from(lax.psum(traces, ('fs', 'tp')))  67.5 us
    dot_general x3, matrix products, local(): jnp.einsum('krs,ksc->krc', poly_rows[:2], cols_in, precision=HIGH)  37.7 us
    slice x3, local copies, waits for them, and re-layouts, gather_turned(): share = result[:, at:at + t[0].size].reshape(-1, *t.shape[1:])  31.3 us
  transfers between devices with their start and end apart: 15, of which 14 were waited for; matrix products, arithmetic and copies ran while one was open for 0% of the time, Pallas kernels for 0%

profile of v1, /device:TPU:1, one launch (start us, length us, event | category | flops | bytes accessed | tf_op | source)
XLA Modules:
  0.0 965.9 jit_solution(4677038367554011040)
XLA Ops:
  8.3 1.4 multiply_add_fusion
  10.9 105.9 %all-gather.19.cloned.1.call-done = f32[2048,1664]{0,1:T(8,128)} async-done(((f32[128,1664]{0,1:T(8,128)}), f32[2048,1664]{0,1:T(8,128)}) %all-gather.19.cloned.1.call-update) | async-done | bytes 13631504 | tf_op jit(solution)/shard_map/all_gather | solution.py:21
  116.8 10.4 %slice.73 = f32[2048,1408]{0,1:T(8,128)} slice(f32[2048,1664]{0,1:T(8,128)} %all-gather.19.cloned.1.call-done), slice={[0:2048], [0:1408]} | slice | bytes 23068672 | tf_op jit(solution)/shard_map/slice | solution.py:23
  127.2 9.2 fusion.25
  136.4 2.8 convolution_bitcast_fusion.2
  139.2 1.9 pad_maximum_fusion
  141.2 33.7 %reduce-scatter.4.cloned.1.call-done = f32[48,2048]{1,0:T(8,128)} async-done(((f32[384,2048]{1,0:T(8,128)}), f32[48,2048]{1,0:T(8,128)}) %reduce-scatter.4.cloned.1.call-update) | async-done | bytes 393232 | tf_op jit(solution)/shard_map/reduce_scatter | solution.py:38
  175.1 31.3 %all-gather.31.cloned.1.call-done = f32[384,2048]{1,0:T(8,128)} async-done(((f32[48,2048]{1,0:T(8,128)}), f32[384,2048]{1,0:T(8,128)}) %all-gather.31.cloned.1.call-update) | async-done | bytes 3145744 | tf_op jit(solution)/shard_map/all_gather | solution.py:41
  206.4 1.8 select_reduce_fusion
  208.3 67.5 %psum.7 = f32[3]{0:T(128)S(1)} all-reduce(f32[3]{0:T(128)S(1)} %get-tuple-element.8), channel_id=1, replica_groups=mesh['fs'=16,'tp'=8] {'fs','tp'}, use_global_device_ids=true, to_apply=%region_2.3 | all-reduce | flops 3 | bytes 24 | tf_op jit(solution)/shard_map/psum | solution.py:76
  275.8 8.2 fusion.10
  284.9 23.8 %all-gather.33.cloned.1.call-done = f32[24,128,256]{2,1,0:T(8,128)} async-done(((f32[3,128,256]{2,1,0:T(8,128)}), f32[24,128,256]{2,1,0:T(8,128)}) %all-gather.33.cloned.1.call-update) | async-done | bytes 3145744 | tf_op jit(solution)/shard_map/all_gather | solution.py:81
  308.7 1.3 slice.76
  310.1 1.7 slice_bitcast_fusion.2
  311.8 1.6 copy.42
  313.7 4.1 fusion.16
  317.9 12.5 %fusion.9 = f32[2,128,704]{1,2,0:T(8,128)S(1)} fusion(f32[2,128,2048]{2,1,0:T(8,128)} %bitcast.90, f32[2,2048,704]{1,2,0:T(8,128)} %bitcast.78, f32[2,128,704]{1,2,0:T(8,128)S(1)} %multiply_add_fusion, f32[2]{0:T(128)S(1)} %bitcast.107), kind=kOutput, calls=%fused_computation.21 | convolution fusion | flops 4429725696 | bytes 15073288 | tf_op jit(solution)/shard_map/krs,ksc->krc/dot_general | solution.py:84
  331.8 101.8 %all-gather.23.cloned.1.call-done = f32[2048,1664]{0,1:T(8,128)} async-done(((f32[128,1664]{0,1:T(8,128)}), f32[2048,1664]{0,1:T(8,128)}) %all-gather.23.cloned.1.call-update) | async-done | bytes 13631504 | tf_op jit(solution)/shard_map/all_gather | solution.py:21
  433.7 10.4 %slice.77 = f32[2048,1408]{0,1:T(8,128)} slice(f32[2048,1664]{0,1:T(8,128)} %all-gather.23.cloned.1.call-done), slice={[0:2048], [0:1408]} | slice | bytes 23068672 | tf_op jit(solution)/shard_map/slice | solution.py:23
  444.1 9.2 fusion.26
  453.3 2.8 convolution_bitcast_fusion.1
  456.1 1.9 pad_maximum_fusion.1
  458.1 33.6 %reduce-scatter.6.cloned.1.call-done = f32[48,2048]{1,0:T(8,128)} async-done(((f32[384,2048]{1,0:T(8,128)}), f32[48,2048]{1,0:T(8,128)}) %reduce-scatter.6.cloned.1.call-update) | async-done | bytes 393232 | tf_op jit(solution)/shard_map/reduce_scatter | solution.py:38
  491.8 31.5 %all-gather.35.cloned.1.call-done = f32[384,2048]{1,0:T(8,128)} async-done(((f32[48,2048]{1,0:T(8,128)}), f32[384,2048]{1,0:T(8,128)}) %all-gather.35.cloned.1.call-update) | async-done | bytes 3145744 | tf_op jit(solution)/shard_map/all_gather | solution.py:41
  523.3 1.8 constant_dynamic-slice_fusion.1
  525.2 61.7 %all-gather.25.cloned.1.call-done = f32[3,2048,256]{2,1,0:T(8,128)} async-done(((f32[3,128,256]{2,1,0:T(8,128)}), f32[3,2048,256]{2,1,0:T(8,128)}) %all-gather.25.cloned.1.call-update) | async-done | bytes 6291472 | tf_op jit(solution)/shard_map/all_gather | solution.py:78
  586.9 8.2 fusion.11
  595.3 27.7 %all-gather.37.cloned.1.call-done = f32[24,128,256]{2,1,0:T(8,128)} async-done(((f32[3,128,256]{2,1,0:T(8,128)}), f32[24,128,256]{2,1,0:T(8,128)}) %all-gather.37.cloned.1.call-update) | async-done | bytes 3145744 | tf_op jit(solution)/shard_map/all_gather | solution.py:81
  623.1 1.3 slice.80
  624.4 1.7 slice_bitcast_fusion.1
  626.4 12.1 %convolution_add_fusion.1 = f32[2,128,704]{1,2,0:T(8,128)S(1)} fusion(f32[2,128,2048]{2,1,0:T(8,128)S(1)} %bitcast.89, f32[2,2048,704]{1,2,0:T(8,128)} %bitcast.82, f32[2,128,704]{1,2,0:T(8,128)S(1)} %fusion.9), kind=kOutput, calls=%fused_computation.19 | convolution fusion | flops 4429545472 | bytes 15073280 | tf_op jit(solution)/shard_map/krs,ksc->krc/dot_general | solution.py:84
  638.8 3.4 fusion.19
  643.4 102.3 %all-gather.27.cloned.1.call-done = f32[2048,1664]{0,1:T(8,128)} async-done(((f32[128,1664]{0,1:T(8,128)}), f32[2048,1664]{0,1:T(8,128)}) %all-gather.27.cloned.1.call-update) | async-done | bytes 13631504 | tf_op jit(solution)/shard_map/all_gather | solution.py:21
  745.7 10.4 %slice.81 = f32[2048,1408]{0,1:T(8,128)} slice(f32[2048,1664]{0,1:T(8,128)} %all-gather.27.cloned.1.call-done), slice={[0:2048], [0:1408]} | slice | bytes 23068672 | tf_op jit(solution)/shard_map/slice | solution.py:23
  756.1 9.2 fusion.27
  765.3 2.8 convolution_bitcast_fusion
  768.1 1.9 pad_maximum_fusion.2
  770.1 33.7 %reduce-scatter.8.cloned.1.call-done = f32[48,2048]{1,0:T(8,128)} async-done(((f32[384,2048]{1,0:T(8,128)}), f32[48,2048]{1,0:T(8,128)}) %reduce-scatter.8.cloned.1.call-update) | async-done | bytes 393232 | tf_op jit(solution)/shard_map/reduce_scatter | solution.py:38
  803.9 31.5 %all-gather.39.cloned.1.call-done = f32[384,2048]{1,0:T(8,128)} async-done(((f32[48,2048]{1,0:T(8,128)}), f32[384,2048]{1,0:T(8,128)}) %all-gather.39.cloned.1.call-update) | async-done | bytes 3145744 | tf_op jit(solution)/shard_map/all_gather | solution.py:41
  835.3 1.8 constant_dynamic-slice_fusion
  837.4 61.3 %all-gather.29.cloned.1.call-done = f32[3,2048,256]{2,1,0:T(8,128)} async-done(((f32[3,128,256]{2,1,0:T(8,128)}), f32[3,2048,256]{2,1,0:T(8,128)}) %all-gather.29.cloned.1.call-update) | async-done | bytes 6291472 | tf_op jit(solution)/shard_map/all_gather | solution.py:78
  898.7 8.2 fusion.12
  906.9 27.9 %all-gather.41.cloned.1.call-done = f32[24,128,256]{2,1,0:T(8,128)} async-done(((f32[3,128,256]{2,1,0:T(8,128)}), f32[24,128,256]{2,1,0:T(8,128)}) %all-gather.41.cloned.1.call-update) | async-done | bytes 3145744 | tf_op jit(solution)/shard_map/all_gather | solution.py:81
  934.9 2.3 slice.84
  937.2 1.7 slice_bitcast_fusion
  939.2 2.5 copy.41
  941.7 13.1 %broadcast_multiply_fusion = (f32[2,128,704]{1,2,0:T(8,128)}, f32[2,128,704]{1,2,0:T(8,128)}) fusion(f32[2,128,704]{1,2,0:T(8,128)S(1)} %copy-done.6, f32[2,128,2048]{2,1,0:T(8,128)S(1)} %bitcast.91, f32[2,2048,704]{1,2,0:T(8,128)} %bitcast.80, f32[2,128,704]{1,2,0:T(8,128)S(1)} %convolution_add_fusion.1), kind=kOutput, calls=%fused_computation.38 | convolution fusion | flops 4430086144 | bytes 16515072 | tf_op jit(solution)/shard_map/krs,ksc->krc/dot_general | solution.py:84
  954.8 4.2 broadcast_multiply_fusion.1
  (64 shorter events, 8.0 us)
Async XLA Ops:
  7.2 109.6 %all-gather.19.cloned.1.call-start = ((), (), s32[]{:S(2)}) async-start(), calls=%async_computation.3 | async-start | bytes 14483456 | tf_op jit(solution)/shard_map/all_gather | solution.py:21
  8.2 305.5 %copy-start.2 = (f32[128,256]{1,0:T(8,128)}, f32[128,256]{1,0:T(8,128)S(1)}, u32[]{:S(2)}) copy-start(f32[128,256]{1,0:T(8,128)S(1)} %multiply_add_fusion.1) | copy-start | bytes 393220
  9.7 308.2 %copy-start = (f32[2,128,704]{1,2,0:T(8,128)}, f32[2,128,704]{1,2,0:T(8,128)S(1)}, u32[]{:S(2)}) copy-start(f32[2,128,704]{1,2,0:T(8,128)S(1)} %multiply_add_fusion) | copy-start | bytes 2162692
  10.8 164.1 %reduce-scatter.4.cloned.1.call-start = ((), (), s32[]{:S(2)}) async-start(), calls=%async_computation.4 | async-start | bytes 3538944 | tf_op jit(solution)/shard_map/reduce_scatter | solution.py:38
  141.2 65.3 %all-gather.31.cloned.1.call-start = ((), (), s32[]{:S(2)}) async-start(), calls=%async_computation.12 | async-start | bytes 3538944 | tf_op jit(solution)/shard_map/all_gather | solution.py:41
  174.9 100.9 %all-gather.21.cloned.1.call-start = ((), (), s32[]{:S(2)}) async-start(), calls=%async_computation.5 | async-start | bytes 6684672 | tf_op jit(solution)/shard_map/all_gather | solution.py:78
  208.2 100.5 %all-gather.33.cloned.1.call-start = ((), (), s32[]{:S(2)}) async-start(), calls=%async_computation.13 | async-start | bytes 3538944 | tf_op jit(solution)/shard_map/all_gather | solution.py:81
  284.1 149.6 %all-gather.23.cloned.1.call-start = ((), (), s32[]{:S(2)}) async-start(), calls=%async_computation.6 | async-start | bytes 14483456 | tf_op jit(solution)/shard_map/all_gather | solution.py:21
  317.8 135.5 %copy-start.3 = (f32[128,256]{1,0:T(8,128)}, f32[128,256]{1,0:T(8,128)S(1)}, u32[]{:S(2)}) copy-start(f32[128,256]{1,0:T(8,128)S(1)} %fusion.16) | copy-start | bytes 393220
  331.4 160.4 %reduce-scatter.6.cloned.1.call-start = ((), (), s32[]{:S(2)}) async-start(), calls=%async_computation.7 | async-start | bytes 3538944 | tf_op jit(solution)/shard_map/reduce_scatter | solution.py:38
  458.1 65.3 %all-gather.35.cloned.1.call-start = ((), (), s32[]{:S(2)}) async-start(), calls=%async_computation.14 | async-start | bytes 3538944 | tf_op jit(solution)/shard_map/all_gather | solution.py:41
  491.8 95.1 %all-gather.25.cloned.1.call-start = ((), (), s32[]{:S(2)}) async-start(), calls=%async_computation.8 | async-start | bytes 6684672 | tf_op jit(solution)/shard_map/all_gather | solution.py:78
  525.1 97.9 %all-gather.37.cloned.1.call-start = ((), (), s32[]{:S(2)}) async-start(), calls=%async_computation.15 | async-start | bytes 3538944 | tf_op jit(solution)/shard_map/all_gather | solution.py:81
  595.1 150.6 %all-gather.27.cloned.1.call-start = ((), (), s32[]{:S(2)}) async-start(), calls=%async_computation.9 | async-start | bytes 14483456 | tf_op jit(solution)/shard_map/all_gather | solution.py:21
  642.3 123.0 %copy-start.4 = (f32[128,256]{1,0:T(8,128)}, f32[128,256]{1,0:T(8,128)S(1)}, u32[]{:S(2)}) copy-start(f32[128,256]{1,0:T(8,128)S(1)} %fusion.19) | copy-start | bytes 393220
  643.4 160.4 %reduce-scatter.8.cloned.1.call-start = ((), (), s32[]{:S(2)}) async-start(), calls=%async_computation.10 | async-start | bytes 3538944 | tf_op jit(solution)/shard_map/reduce_scatter | solution.py:38
  770.1 65.3 %all-gather.39.cloned.1.call-start = ((), (), s32[]{:S(2)}) async-start(), calls=%async_computation.16 | async-start | bytes 3538944 | tf_op jit(solution)/shard_map/all_gather | solution.py:41
  803.8 94.9 %all-gather.29.cloned.1.call-start = ((), (), s32[]{:S(2)}) async-start(), calls=%async_computation.11 | async-start | bytes 6684672 | tf_op jit(solution)/shard_map/all_gather | solution.py:78
  837.1 97.8 %all-gather.41.cloned.1.call-start = ((), (), s32[]{:S(2)}) async-start(), calls=%async_computation.17 | async-start | bytes 3538944 | tf_op jit(solution)/shard_map/all_gather | solution.py:81
  938.9 2.8 copy-start.6
  941.7 13.1 %copy-start.1 = (f32[1,128,8,256]{1,3,2,0:T(8,128)S(1)}, f32[1,128,8,256]{1,3,2,0:T(8,128)}, u32[]{:S(2)}) copy-start(f32[1,128,8,256]{1,3,2,0:T(8,128)} %copy.41) | copy-start | bytes 3145732
  941.7 13.1 %copy-start.5 = (f32[128,256]{1,0:T(8,128)S(1)}, f32[128,256]{1,0:T(8,128)}, u32[]{:S(2)}) copy-start(f32[128,256]{1,0:T(8,128)} %copy-done.4) | copy-start | bytes 393220
  941.7 13.1 %copy-start.7 = (f32[128,256]{1,0:T(8,128)S(1)}, f32[128,256]{1,0:T(8,128)}, u32[]{:S(2)}) copy-start(f32[128,256]{1,0:T(8,128)} %param.7) | copy-start | bytes 393220
Sparse Core Ops, SparseCore 0:
  11.0 105.7 all-gather.18
  141.3 33.5 reduce-scatter.3
  176.6 29.8 all-gather.30
  209.0 61.4 all-gather.20
  284.2 24.4 all-gather.32
  331.5 102.1 all-gather.22
  458.2 33.5 reduce-scatter.5
  493.4 29.8 all-gather.34
  526.1 60.7 all-gather.24
  595.2 27.7 all-gather.36
  643.5 102.1 all-gather.26
  770.2 33.5 reduce-scatter.7
  805.5 29.8 all-gather.38
  837.9 60.7 all-gather.28
  907.1 27.7 all-gather.40
